TPU v7x, 512 devices: a whole 4x4x16 slice. The times are simulated.
512 devices in a mesh: sp: 64 (over z, y), tp: 8 (over x, core).
Axes of the slice: x: 4, y: 4, z: 16, core: 2. Of those that a mesh axis runs over, the one named last changes fastest.
Arguments:
- tokens: bfloat16 [16384, 4096], P('sp'), may hold values from -5 to 5
- documents: int32 [16384], P('sp'), may hold values from 0 to 15, never falling along the last dimension, each value on 1 to 2048 neighbouring positions
- norm_gain: float32 [2, 4096], replicated, may hold values from 0.1 to 1.9
- in_weight: bfloat16 [2, 4096, 2048], P(None, 'sp', 'tp'), may hold values from -0.09375 to 0.09375
- conv_taps: float32 [2, 4, 2048], P(None, None, 'tp'), may hold values from -3 to 3
- conv_bias: float32 [2, 2048], P(None, 'tp'), may hold values from -0.75 to 0.75
- recur_gate: bfloat16 [2, 32, 64, 64], P(None, 'tp'), may hold values from -0.75 to 0.75
- input_gate: bfloat16 [2, 32, 64, 64], P(None, 'tp'), may hold values from -0.75 to 0.75
- recur_bias: float32 [2, 2048], P(None, 'tp'), may hold values from -4 to 4
- input_bias: float32 [2, 2048], P(None, 'tp'), may hold values from -4 to 4
- decay_param: float32 [2, 2048], P(None, 'tp'), may hold values from 4 to 7
- out_weight: bfloat16 [2, 2048, 4096], P(None, 'tp', 'sp'), may hold values from -0.375 to 0.375
Outputs:
- layered: bfloat16 [16384, 4096], P('sp')
All inputs are finite; a program needn't handle non-finite values.
Results may differ from a plain program's by a relative error of at most 0.017.
Values may be sent and summed in bfloat16 or wider, within the bound.
A program may use at most 64 MiB of HBM per device.

v0:
```python
import jax
import jax.numpy as jnp
from jax import lax
from jax.sharding import PartitionSpec as P

RG_C = 8.0
EPS = 0.1


def gather_turned(arrays, axis, dims):
    turned = [jnp.moveaxis(a, dim, 0) for a, dim in zip(arrays, dims)]
    both = jnp.concatenate([t.reshape(len(t), -1) for t in turned], axis=1)
    result, at, finished = (lax.all_gather(both, axis, axis=0, tiled=True), 0, [])
    for t, dim in zip(turned, dims):
        piece = result[:, at : at + t[0].size].reshape(-1, *t.shape[1:])
        finished.append(jnp.moveaxis(piece, 0, dim))
        at += t[0].size
    return tuple(finished)


def passed_along(block, axis, distance):
    devices = range(lax.axis_size(axis))
    route = [(i - distance, i) for i in devices if i - distance in devices]
    return lax.ppermute(block, axis, route)


def from_everyone(x, axis):
    copies = jnp.broadcast_to(x, (lax.axis_size(axis), *x.shape))
    return lax.all_to_all(copies, axis, split_axis=0, concat_axis=0, tiled=True)


def all_in_one(x, axis):
    leaves = jax.tree.leaves(x)
    order = sorted(range(len(leaves)), key=lambda k: -leaves[k].size)
    width = (1, *leaves[order[0]].shape)[-1]
    lines = [
        jnp.pad(leaves[k].reshape(-1), (0, -leaves[k].size % width)).reshape(-1, width)
        for k in order
    ]
    both, at, found = (from_everyone(jnp.concatenate(lines), axis), 0, {})
    for k, line in zip(order, lines):
        piece = both[:, at : at + len(line)].reshape(len(both), -1)
        found[k] = piece[:, : leaves[k].size].reshape(-1, *leaves[k].shape)
        at += len(line)
    numbers = iter(range(len(leaves)))
    return jax.tree.map(lambda _: found[next(numbers)], x)


def folded_in_pairs(pieces, combine):
    while len(jax.tree.leaves(pieces)[0]) > 1:
        pieces = jax.vmap(combine)(
            *(jax.tree.map(lambda part: part[side::2], pieces) for side in (0, 1))
        )
    return jax.tree.map(lambda part: part[0], pieces)


def carried_in(x, axis, combine, identity):
    peers, index = (lax.axis_size(axis), lax.axis_index(axis))
    passed = jnp.arange(peers) < index

    def kept(part, zero, own):
        part = jnp.where(
            passed.reshape(-1, *(1 for _ in own.shape)), part, jnp.asarray(zero, own.dtype)
        )
        return part

    pieces = all_in_one(x, axis)
    return folded_in_pairs(jax.tree.map(kept, pieces, identity, x), combine)


def norm_rows(values_in, gain_row):
    values = values_in.astype(jnp.float32)
    scaled = values * lax.rsqrt(jnp.mean(values * values, axis=-1, keepdims=True) + EPS)
    return (scaled * gain_row[None, :]).astype(jnp.bfloat16)


def combine(earlier, following):
    return (earlier[0] * following[0], following[0] * earlier[1] + following[1])


def per_device(
    tokens,
    documents,
    norm_gain,
    in_weight,
    conv_taps,
    conv_bias,
    recur_gate,
    input_gate,
    recur_bias,
    input_bias,
    decay_param,
    out_weight,
):
    num_rows = tokens.shape[0]
    layer_count = in_weight.shape[0]
    chan_width = in_weight.shape[2]
    tap_count = conv_taps.shape[1]
    blocks = recur_gate.shape[1]
    block_dim = recur_gate.shape[2]
    doc_values = documents.astype(jnp.bfloat16)
    whole_in, whole_out = gather_turned((in_weight, out_weight), "sp", (1, 2))
    state_x = tokens
    for depth_at in range(layer_count):
        normed = norm_rows(state_x, norm_gain[depth_at])
        projected = jnp.dot(normed, whole_in[depth_at], preferred_element_type=jnp.float32)
        mixed_in = projected.astype(jnp.bfloat16)
        cut_at = num_rows - tap_count + 1
        tail_in, tail_doc = passed_along((mixed_in[cut_at:], doc_values[cut_at:]), "sp", 1)
        ext_in = jnp.concatenate([tail_in, mixed_in], axis=0).astype(jnp.float32)
        ext_doc = jnp.concatenate([tail_doc, doc_values], axis=0)
        first = tap_count - 1
        conv_sum = conv_bias[depth_at][None, :] + conv_taps[depth_at, 0][None, :] * ext_in[first:]
        for lag_step in range(1, tap_count):
            low = first - lag_step
            same_doc = (ext_doc[low : low + num_rows] == doc_values)[:, None]
            conv_sum = conv_sum + jnp.where(
                same_doc, conv_taps[depth_at, lag_step][None, :] * ext_in[low : low + num_rows], 0.0
            )
        conv_out = conv_sum.astype(jnp.bfloat16)
        grouped = conv_out.reshape(num_rows, blocks, block_dim)
        recur_rate = jax.nn.sigmoid(
            jnp.einsum(
                "snb,nbc->snc", grouped, recur_gate[depth_at], preferred_element_type=jnp.float32
            ).reshape(num_rows, chan_width)
            + recur_bias[depth_at][None, :]
        )
        input_rate = jax.nn.sigmoid(
            jnp.einsum(
                "snb,nbc->snc", grouped, input_gate[depth_at], preferred_element_type=jnp.float32
            ).reshape(num_rows, chan_width)
            + input_bias[depth_at][None, :]
        )
        reset = ext_doc[first - 1 : first - 1 + num_rows] != doc_values
        log_decay = -RG_C * jax.nn.softplus(-decay_param[depth_at])[None, :] * recur_rate
        decay_now = jnp.where(reset[:, None], 0.0, jnp.exp(log_decay))
        drive_term = jnp.sqrt(jnp.maximum(-jnp.expm1(2.0 * log_decay), 0.0)) * (
            input_rate * conv_out.astype(jnp.float32)
        )
        cum_decay, local_state = lax.associative_scan(combine, (decay_now, drive_term), axis=0)
        identity = (jnp.ones((chan_width,), jnp.float32), jnp.zeros((chan_width,), jnp.float32))
        _, carried = carried_in(
            (cum_decay[num_rows - 1], local_state[num_rows - 1]), "sp", combine, identity
        )
        hidden = (local_state + cum_decay * carried[None, :]).astype(jnp.bfloat16)
        partial_sum = jnp.dot(hidden, whole_out[depth_at], preferred_element_type=jnp.float32)
        summed = lax.psum(partial_sum.astype(jnp.bfloat16), "tp").astype(jnp.float32)
        state_x = (state_x.astype(jnp.float32) + summed).astype(jnp.bfloat16)
    return state_x


def solution(mesh):
    return jax.shard_map(
        per_device,
        mesh=mesh,
        in_specs=(
            P("sp", None),
            P("sp"),
            P(),
            P(None, "sp", "tp"),
            P(None, None, "tp"),
            P(None, "tp"),
            P(None, "tp", None, None),
            P(None, "tp", None, None),
            P(None, "tp"),
            P(None, "tp"),
            P(None, "tp"),
            P(None, "tp", "sp"),
        ),
        out_specs=P("sp", None),
        check_vma=False,
    )
```

profile of v0, /device:TPU:1, one launch (start us, length us, event | category | flops | bytes accessed | tf_op | source)
XLA Modules:
  0.0 457.6 jit_solution(3005989956827685192)
XLA Ops:
  9.7 4.0 collective-permute-start.1
  13.7 2.1 fusion
  15.8 1.3 fusion.96
  17.1 1.4 fusion.76
  18.5 1.4 fusion.95
  19.9 1.3 fusion.94
  21.2 1.5 fusion.87
  22.7 1.5 fusion.83
  24.2 139.7 %all-gather.2.cloned.1.call-done = bf16[4096,1024]{1,0:T(8,128)(2,1)} async-done(((bf16[64,1024]{1,0:T(8,128)(2,1)}), bf16[4096,1024]{1,0:T(8,128)(2,1)}) %all-gather.2.cloned.1.call-update) | async-done | bytes 8388624 | tf_op jit(solution)/shard_map/all_gather | solution.py:13
  164.0 5.2 %fusion.78 = (bf16[4096,512]{1,0:T(8,128)(2,1)S(1)}, bf16[4096,512]{1,0:T(8,128)(2,1)}) fusion(bf16[4096,1024]{1,0:T(8,128)(2,1)} %all-gather.2.cloned.1.call-done), kind=kLoop, calls=%fused_computation.223 | loop fusion | bytes 16777216 | tf_op jit(solution)/shard_map/slice | solution.py:15
  169.5 2.1 copy-done
  172.4 1.7 collective-permute-start
  201.7 12.3 %all-to-all-start = ((f32[64,2,256]{2,1,0:T(2,128)}), f32[64,2,256]{2,1,0:T(2,128)S(1)}, u32[]{:S(2)}, u32[]{:S(2)}) async-start(f32[64,2,256]{2,1,0:T(2,128)} %broadcast_in_dim.100), calls=%async_computation | async-start | bytes 262144 | tf_op jit(solution)/shard_map/all_to_all | solution.py:29
  214.1 6.5 %copy.56 = bf16[4096,512]{0,1:T(8,128)(2,1)} copy(bf16[4096,512]{1,0:T(8,128)(2,1)} %get-tuple-element.6) | data formatting | bytes 8388608 | tf_op jit(solution)/shard_map/reshape | solution.py:15
  220.5 8.4 %all-to-all-done = f32[64,2,256]{2,1,0:T(2,128)S(1)} async-done(((f32[64,2,256]{2,1,0:T(2,128)}), f32[64,2,256]{2,1,0:T(2,128)S(1)}, u32[]{:S(2)}, u32[]{:S(2)}) %all-to-all-start) | async-done | bytes 131104 | tf_op jit(solution)/shard_map/all_to_all | solution.py:29
  229.7 3.6 convolution_convert_fusion.1
  233.4 81.6 %all-reduce.67.cloned.1.call-done = bf16[256,4096]{1,0:T(8,128)(2,1)} async-done(((bf16[256,4096]{1,0:T(8,128)(2,1)}), bf16[256,4096]{1,0:T(8,128)(2,1)}) %all-reduce.67.cloned.1.call-update) | async-done | bytes 2097168 | tf_op jit(solution)/shard_map/psum | solution.py:147
  314.9 2.5 fusion.4
  317.6 2.6 fusion.19
  320.2 3.1 collective-permute-start.2
  337.4 31.6 %all_to_all.10 = f32[64,2,256]{2,1,0:T(2,128)S(1)} all-to-all(f32[64,2,256]{2,1,0:T(2,128)S(1)} %broadcast_in_dim.103), channel_id=1, replica_groups=mesh['sp'=64,'tp'=8] {'sp'}, dimensions={0} | all-to-all | bytes 262144 | tf_op jit(solution)/shard_map/all_to_all | solution.py:29
  369.6 3.6 convolution_convert_fusion
  373.3 73.1 %all-reduce.69.cloned.1.call-done = bf16[256,4096]{1,0:T(8,128)(2,1)} async-done(((bf16[256,4096]{1,0:T(8,128)(2,1)}), bf16[256,4096]{1,0:T(8,128)(2,1)}) %all-reduce.69.cloned.1.call-update) | async-done | bytes 2097168 | tf_op jit(solution)/shard_map/psum | solution.py:147
  446.3 4.7 %fusion.7 = bf16[256,4096]{1,0:T(8,128)(2,1)} fusion(bf16[256,4096]{1,0:T(8,128)(2,1)} %all-reduce.69.cloned.1.call-done, bf16[256,4096]{1,0:T(8,128)(2,1)} %all-reduce.67.cloned.1.call-done, bf16[256,4096]{1,0:T(8,128)(2,1)S(1)} %copy-done), kind=kLoop, calls=%fused_computation.15 | loop fusion | flops 8388608 | bytes 8388608 | tf_op jit(solution)/shard_map/convert_element_type | solution.py:148
  (402 shorter events, 46.2 us)
Async XLA Ops:
  6.5 157.4 %all-gather.2.cloned.1.call-start = ((), (), s32[]{:S(2)}) async-start(), calls=%async_computation.2 | async-start | bytes 8519680 | tf_op jit(solution)/shard_map/all_gather | solution.py:13
  9.7 14.5 %collective-permute-start.1 = (bf16[3]{0:T(256)(128)(2,1)S(1)}, bf16[3]{0:T(256)(128)(2,1)S(1)}, u32[]{:S(2)}, u32[]{:S(2)}) collective-permute-start(bf16[3]{0:T(256)(128)(2,1)S(1)} %slice.768), channel_id=1, source_target_pairs={{0,8},{8,16},{16,24},{24,32},{32,40},{40,48},{48,56},{56,64},{64,7... | collective-permute-start | bytes 26 | tf_op jit(solution)/shard_map/ppermute | solution.py:24
  17.1 157.8 %copy-start.22 = (f32[1,256]{1,0:T(1,128)}, f32[1,256]{1,0:T(1,128)S(1)}, u32[]{:S(2)}) copy-start(f32[1,256]{1,0:T(1,128)S(1)} %get-tuple-element.110) | copy-start | bytes 3076
  22.7 152.2 %copy-start.17 = (f32[1,1,256]{2,1,0:T(1,128)}, f32[1,1,256]{2,1,0:T(1,128)S(1)}, u32[]{:S(2)}) copy-start(f32[1,1,256]{2,1,0:T(1,128)S(1)} %get-tuple-element.65) | copy-start | bytes 3076
  22.7 152.2 %copy-start.18 = (f32[1,1,256]{2,1,0:T(1,128)}, f32[1,1,256]{2,1,0:T(1,128)S(1)}, u32[]{:S(2)}) copy-start(f32[1,1,256]{2,1,0:T(1,128)S(1)} %get-tuple-element.66) | copy-start | bytes 3076
  22.7 152.2 %copy-start.19 = (f32[1,1,256]{2,1,0:T(1,128)}, f32[1,1,256]{2,1,0:T(1,128)S(1)}, u32[]{:S(2)}) copy-start(f32[1,1,256]{2,1,0:T(1,128)S(1)} %get-tuple-element.67) | copy-start | bytes 3076
  22.7 152.2 %copy-start.20 = (f32[1,1,256]{2,1,0:T(1,128)}, f32[1,1,256]{2,1,0:T(1,128)S(1)}, u32[]{:S(2)}) copy-start(f32[1,1,256]{2,1,0:T(1,128)S(1)} %get-tuple-element.68) | copy-start | bytes 3076
  172.4 2.4 collective-permute-start
  193.9 6.8 %copy-start.24 = (f32[1,256]{1,0:T(1,128)S(1)}, f32[1,256]{1,0:T(1,128)}, u32[]{:S(2)}) copy-start(f32[1,256]{1,0:T(1,128)} %slice.1037) | copy-start | bytes 3076
  193.9 6.9 %copy-start.23 = (f32[1,256]{1,0:T(1,128)S(1)}, f32[1,256]{1,0:T(1,128)}, u32[]{:S(2)}) copy-start(f32[1,256]{1,0:T(1,128)} %slice.1011) | copy-start | bytes 3076
  201.7 27.3 %all-to-all-start = ((f32[64,2,256]{2,1,0:T(2,128)}), f32[64,2,256]{2,1,0:T(2,128)S(1)}, u32[]{:S(2)}, u32[]{:S(2)}) async-start(f32[64,2,256]{2,1,0:T(2,128)} %broadcast_in_dim.100), calls=%async_computation | async-start | bytes 262144 | tf_op jit(solution)/shard_map/all_to_all | solution.py:29
  214.0 100.9 %all-reduce.67.cloned.1.call-start = ((), (), s32[]{:S(2)}) async-start(), calls=%async_computation.3 | async-start | bytes 4194304 | tf_op jit(solution)/shard_map/psum | solution.py:147
  214.1 15.0 %copy-start.25 = (pred[64]{0:T(512)(128)(4,1)}, pred[64]{0:T(512)(128)(4,1)S(1)}, u32[]{:S(2)}) copy-start(pred[64]{0:T(512)(128)(4,1)S(1)} %iota_compare_fusion) | copy-start | bytes 196
  233.3 84.2 %copy-start.6 = (f32[1,4096]{1,0:T(1,128)S(1)}, f32[1,4096]{1,0:T(1,128)}, u32[]{:S(2)}) copy-start(f32[1,4096]{1,0:T(1,128)} %get-tuple-element.44) | copy-start | bytes 49156
  233.3 213.0 %all-reduce.69.cloned.1.call-start = ((), (), s32[]{:S(2)}) async-start(), calls=%async_computation.4 | async-start | bytes 4194304 | tf_op jit(solution)/shard_map/psum | solution.py:147
  317.5 6.4 %copy-start.8 = (pred[256]{0:T(512)(128)(4,1)S(1)}, pred[256]{0:T(512)(128)(4,1)}, u32[]{:S(2)}) copy-start(pred[256]{0:T(512)(128)(4,1)} %copy-done.7) | copy-start | bytes 772
  317.5 6.4 %copy-start.10 = (pred[256]{0:T(512)(128)(4,1)S(1)}, pred[256]{0:T(512)(128)(4,1)}, u32[]{:S(2)}) copy-start(pred[256]{0:T(512)(128)(4,1)} %copy-done.9) | copy-start | bytes 772
  317.5 6.4 %copy-start.12 = (pred[256]{0:T(512)(128)(4,1)S(1)}, pred[256]{0:T(512)(128)(4,1)}, u32[]{:S(2)}) copy-start(pred[256]{0:T(512)(128)(4,1)} %copy-done.11) | copy-start | bytes 772
  317.5 6.4 %copy-start.13 = (f32[1,1,256]{2,1,0:T(1,128)S(1)}, f32[1,1,256]{2,1,0:T(1,128)}, u32[]{:S(2)}) copy-start(f32[1,1,256]{2,1,0:T(1,128)} %get-tuple-element.63) | copy-start | bytes 3076
  317.5 6.4 %copy-start.14 = (f32[1,1,256]{2,1,0:T(1,128)S(1)}, f32[1,1,256]{2,1,0:T(1,128)}, u32[]{:S(2)}) copy-start(f32[1,1,256]{2,1,0:T(1,128)} %get-tuple-element.64) | copy-start | bytes 3076
  317.5 6.4 %copy-start.15 = (f32[1,1,256]{2,1,0:T(1,128)S(1)}, f32[1,1,256]{2,1,0:T(1,128)}, u32[]{:S(2)}) copy-start(f32[1,1,256]{2,1,0:T(1,128)} %get-tuple-element.69) | copy-start | bytes 3076
  317.5 6.9 %copy-start.5 = (bf16[2,4,64,64]{3,2,1,0:T(8,128)(2,1)S(1)}, bf16[2,4,64,64]{3,2,1,0:T(8,128)(2,1)}, u32[]{:S(2)}) copy-start(bf16[2,4,64,64]{3,2,1,0:T(8,128)(2,1)} %param.19) | copy-start | bytes 196612
  320.2 3.6 collective-permute-start.2
  333.7 35.4 %copy-start.26 = (pred[64]{0:T(512)(128)(4,1)S(1)}, pred[64]{0:T(512)(128)(4,1)}, u32[]{:S(2)}) copy-start(pred[64]{0:T(512)(128)(4,1)} %copy-done.25) | copy-start | bytes 196
  (11 other events, 43.7 us)
Sparse Core Ops, SparseCore 0:
  10.3 153.6 all-gather.1
  233.4 81.4 all-reduce.66
  373.4 72.8 all-reduce.68
where the time goes:
time: 460 us; the launch traced here: 458 us
  waiting for transfers between devices  303 us (66%)
  local copies, waits for them, and re-layouts  43.1 us (9%)
  other arithmetic  32.1 us (7%)
  blocking collectives  31.6 us (7%)
  starting transfers between devices  21.2 us (5%)
  between operations  14.7 us (3%)
  matrix products  11.5 us (2%)
    psum x2, waiting for transfers between devices, per_device(): lax.psum(partial_sum.astype(jnp.bfloat16), 'tp').astype(jnp.float32)  155 us
    all_gather x1, waiting for transfers between devices, gather_turned(): lax.all_gather(both, axis, axis=0, tiled=True)  140 us
    all_to_all x1, blocking collectives, from_everyone(): return lax.all_to_all(copies, axis, split_axis=0, concat_axis=0, tiled=True)  31.6 us
    slice x104, local copies, waits for them, and re-layouts, per_device(): lax.associative_scan(combine, (decay_now, drive_term), axis=0)  15.8 us
    all_to_all x1, starting transfers between devices, from_everyone(): return lax.all_to_all(copies, axis, split_axis=0, concat_axis=0, tiled=True)  12.3 us
    concatenate x27, other arithmetic, per_device(): lax.associative_scan(combine, (decay_now, drive_term), axis=0)  11.6 us
  transfers between devices with their start and end apart: 7, of which 6 were waited for; matrix products, arithmetic and copies ran while one was open for 4% of the time, Pallas kernels for 0%

commit v1 on v0

v1 whole, which is shorter than its diff:
```python
import functools

import jax
import jax.numpy as jnp
from jax import lax
from jax.experimental import pallas as pl
from jax.experimental.pallas import tpu as pltpu
from jax.sharding import PartitionSpec as P

RG_C = 8.0
EPS = 0.1
MESH = pl.DeviceIdType.MESH
F32 = jnp.float32
BF16 = jnp.bfloat16
NY = 4
NX = 4
BACK = 8
OFFSETS = (0, 4, 8, 12)


def nt_dot(a, b):
    return lax.dot_general(a, b, (((1,), (1,)), ((), ())), preferred_element_type=F32)


def kernel(
    n_sp, docs, tokens, gain, w_in, taps, conv_bias, rgate, igate, rbias, ibias, decay, w_out, out,
    wbuf, pdoc, dext, masks, gm, xg, x1, outb, acc, ss, ext, tail, a_s, b_s, h_s, p_s, hid,
    cown, cbuf, send_d, recv_d, send_x, recv_x, keep, own,
    z_recv, y_recv, z_send, y_send, d_sem, t_sem, c_recv, c_send, dr, ds, xr, xs, gr, gs, pr, ps, o_sem,
):
    rows, width = tokens.shape
    chans = taps.shape[2]
    blk = w_in.shape[1]
    half_l = chans // 2
    n_tp = 2 * NX
    cw = width // n_tp
    hr = rows // 2
    segs = 8
    steps = rows // segs
    n_z = n_sp // NY
    sp = lax.axis_index("sp")
    tp = lax.axis_index("tp")
    z, y = sp // NY, lax.rem(sp, NY)
    x, core = tp // 2, lax.rem(tp, 2)

    def at_y(d):
        return z * NY + lax.rem(y + d + NY, NY)

    def at_z(d):
        return lax.rem(z + d + n_z, n_z) * NY + y

    def at_sp(d):
        return lax.rem(sp + d + n_sp, n_sp)

    def at_x(d, c=0):
        return lax.rem(x + d + NX, NX) * 2 + (core if c == 0 else 1 - core)

    partner = x * 2 + (1 - core)
    xp, xm = at_x(1), at_x(-1)

    def rcopy(src, dst, ssem, rsem, to_sp, to_tp):
        pltpu.make_async_remote_copy(
            src_ref=src, dst_ref=dst, send_sem=ssem, recv_sem=rsem,
            device_id=(to_sp, to_tp), device_id_type=MESH,
        ).start()

    def wait(ref, sem):
        pltpu.make_async_copy(ref, ref, sem).wait()

    barrier = pltpu.get_barrier_semaphore()
    partners = [(at_y(1), tp), (at_y(-1), tp), (at_y(2), tp), (at_z(1), tp), (at_z(-1), tp)]
    partners += [(sp, xp), (sp, xm), (sp, partner)]
    partners += [(at_sp(d), tp) for k in range(1, BACK + 1) for d in (k, -k)]
    for to_sp, to_tp in partners:
        pl.semaphore_signal(barrier, inc=1, device_id=(to_sp, to_tp), device_id_type=MESH)

    eye = (
        lax.broadcasted_iota(jnp.int32, (blk, blk), 0) == lax.broadcasted_iota(jnp.int32, (blk, blk), 1)
    ).astype(BF16)
    mine = pl.ds(pl.multiple_of(sp * blk, blk), blk)
    for layer in range(2):
        w = w_in[layer]
        wt = nt_dot(eye, w_out[layer]).astype(BF16)
        for h in range(2):
            lanes = slice(h * half_l, (h + 1) * half_l)
            wbuf[2 * layer, h, mine, :] = w[:, lanes]
            wbuf[2 * layer + 1, h, mine, :] = wt[:, lanes]

    pl.semaphore_wait(barrier, len(partners))

    def block_rows(zz, yy):
        return pl.ds(pl.multiple_of((zz * NY + yy) * blk, blk), blk)

    def z_rows(zz):
        return pl.ds(pl.multiple_of(zz * NY * blk, NY * blk), NY * blk)

    def last_step(m, d):
        full = n_z // 2
        return full if (m + d) % 2 == 0 else full - 1

    def start_y(m):
        for d in (1, -1, 2):
            for h in range(2):
                piece = wbuf.at[m, h, mine, :]
                rcopy(piece, piece, y_send.at[m], y_recv.at[m, h], at_y(d), tp)

    def pass_first(m, d, zz):
        to = at_z(1 if d == 0 else -1)
        s_sem = z_send.at[m]
        return to, s_sem

    def fwd_first(m, d, s, zz):
        to, s_sem = pass_first(m, d, zz)
        r = block_rows(zz, y)
        piece = wbuf.at[m, :, r, :] if m == 0 else wbuf.at[m, 1, r, :]
        rcopy(piece, piece, s_sem, z_recv.at[m, d, s, 0], to, tp)

    def fwd_second(m, d, s, zz):
        to, s_sem = pass_first(m, d, zz)
        if m == 0:
            for dy in (1, -1, 2):
                piece = wbuf.at[m, 0, block_rows(zz, lax.rem(y + dy + NY, NY)), :]
                rcopy(piece, piece, s_sem, z_recv.at[m, d, s, 1], to, tp)
        else:
            piece = wbuf.at[m, 0, z_rows(zz), :]
            rcopy(piece, piece, s_sem, z_recv.at[m, d, s, 1], to, tp)

    first_rows = [2 * blk, blk, blk, blk]
    second_rows = [3 * blk, 4 * blk, 4 * blk, 4 * blk]

    def tick(m, s):
        if s == 0:
            for d in range(2):
                fwd_first(m, d, 1, z)
            start_y(m)
            wait(wbuf.at[m, 0, 0 : 3 * blk], y_recv.at[m, 0])
            for d in range(2):
                fwd_second(m, d, 1, z)
            return
        live = [d for d in range(2) if s <= last_step(m, d)]
        zs = {0: lax.rem(z - s + n_z, n_z), 1: lax.rem(z + s, n_z)}
        for d in live:
            wait(wbuf.at[m, 0, 0 : first_rows[m]], z_recv.at[m, d, s, 0])
            if s < last_step(m, d):
                fwd_first(m, d, s + 1, zs[d])
            piece = wbuf.at[m, 1, block_rows(zs[d], y), :]
            for dy in (1, -1, 2):
                rcopy(piece, piece, y_send.at[m], y_recv.at[m, 1], at_y(dy), tp)
        for d in live:
            wait(wbuf.at[m, 0, 0 : second_rows[m]], z_recv.at[m, d, s, 1])
            if s < last_step(m, d):
                fwd_second(m, d, s + 1, zs[d])

    done = [0]

    def run_ticks(upto):
        while done[0] < upto:
            t = done[0]
            for m in range(4):
                if 0 <= t - OFFSETS[m] <= n_z // 2:
                    tick(m, t - OFFSETS[m])
            done[0] += 1

    def have(m):
        run_ticks(OFFSETS[m] + n_z // 2 + 1)
        wait(wbuf.at[m, 0, 0 : (n_z * 3) * blk], y_recv.at[m, 1])

    def wrows(m, q):
        r = pl.ds(pl.multiple_of(q * cw, cw), cw)
        return jnp.concatenate([wbuf[m, 0, r, :], wbuf[m, 1, r, :]], axis=1)

    rcopy(docs, pdoc, d_sem.at[0], d_sem.at[1], at_sp(1), tp)
    run_ticks(1)

    ss[...] = jnp.zeros_like(ss)
    acc[...] = jnp.zeros_like(acc)

    def scaled(layer, values, q):
        v = values.astype(F32)
        sq = v * v
        part = sq[:, 0:128]
        for i in range(1, cw // 128):
            part = part + sq[:, i * 128 : (i + 1) * 128]
        ss[...] += part
        g = gain[layer : layer + 1, pl.ds(pl.multiple_of(q * cw, cw), cw)]
        return (v * g).astype(BF16)

    def prepare(q, _):
        xg[q] = scaled(0, tokens[:, pl.ds(pl.multiple_of(q * cw, cw), cw)], q)
        return 0

    lax.fori_loop(0, n_tp, prepare, 0)
    run_ticks(2)

    bd = rgate.shape[2]
    spread = (
        lax.rem(lax.broadcasted_iota(jnp.int32, (bd, chans), 1), bd)
        == lax.broadcasted_iota(jnp.int32, (bd, chans), 0)
    ).astype(BF16)
    on_block = (
        lax.broadcasted_iota(jnp.int32, (chans, chans), 0) // bd
        == lax.broadcasted_iota(jnp.int32, (chans, chans), 1) // bd
    )
    for layer in range(2):
        for i, g in enumerate((rgate, igate)):
            tiled = jnp.dot(g[layer], spread, preferred_element_type=F32)
            gm[layer, :, i * chans : (i + 1) * chans] = jnp.where(on_block, tiled, 0.0).astype(BF16)
    run_ticks(3)

    wait(pdoc, d_sem.at[1])
    eye_r = (
        lax.broadcasted_iota(jnp.int32, (rows, rows), 0) == lax.broadcasted_iota(jnp.int32, (rows, rows), 1)
    ).astype(BF16)
    own_docs = jnp.broadcast_to(docs[...], (128, rows)).astype(F32).astype(BF16)
    prev_docs = jnp.broadcast_to(pdoc[...], (128, rows)).astype(F32).astype(BF16)
    dext[8:, :] = nt_dot(eye_r, own_docs)
    before = nt_dot(eye_r[rows - 8 :, :], prev_docs)
    first_dev = jnp.broadcast_to((sp == 0).astype(F32), (8, 128))
    dext[0:8, :] = before * (1.0 - first_dev) - first_dev
    for k in range(1, 4):
        masks[k - 1] = (dext[8 - k : 8 - k + rows, :] == dext[8:, :]).astype(F32)

    def put(ref, value):
        for i in range(chans // 128):
            ref[i] = value[:, i * 128 : (i + 1) * 128]

    def across(ref, j):
        return jnp.concatenate(
            [ref[i, pl.ds(j, segs, stride=steps), :] for i in range(chans // 128)], axis=1
        )

    def layer_front(layer):
        r = lax.rsqrt(jnp.sum(ss[...], axis=1, keepdims=True) * (1.0 / width) + EPS)
        mixed = (acc[...] * r).astype(BF16).astype(F32)
        ext[8:, :] = mixed
        rcopy(ext.at[rows : rows + 8, :], tail.at[layer], t_sem.at[layer, 0], t_sem.at[layer, 1], at_sp(1), tp)
        wait(tail.at[layer], t_sem.at[layer, 1])
        wait(tail.at[layer], t_sem.at[layer, 0])
        ext[0:8, :] = tail[layer]

        def wide(mask):
            return jnp.concatenate([mask] * (chans // 128), axis=1)

        conv = conv_bias[layer : layer + 1, :] + taps[layer, 0:1, :] * mixed
        for k in range(1, 4):
            conv = conv + wide(masks[k - 1]) * (taps[layer, k : k + 1, :] * ext[8 - k : 8 - k + rows, :])
        conv_b = conv.astype(BF16)
        conv_f = conv_b.astype(F32)
        logits = jnp.dot(conv_b, gm[layer], preferred_element_type=F32)
        rr = jax.nn.sigmoid(logits[:, :chans] + rbias[layer : layer + 1, :])
        ir = jax.nn.sigmoid(logits[:, chans:] + ibias[layer : layer + 1, :])
        dp = decay[layer : layer + 1, :]
        soft = jnp.maximum(-dp, 0.0) + jnp.log1p(jnp.exp(-jnp.abs(dp)))
        log_decay = (-RG_C * soft) * rr
        put(a_s, jnp.exp(log_decay) * wide(masks[0]))
        u = -2.0 * log_decay
        series = 1.0 - u * (1.0 / 8.0)
        for n in (7, 6, 5, 4, 3, 2):
            series = 1.0 - (u * (1.0 / n)) * series
        gone = jnp.where(u < 0.35, u * series, 1.0 - jnp.exp(-u))
        put(b_s, jnp.sqrt(jnp.maximum(gone, 0.0)) * (ir * conv_f))
        h = jnp.zeros((segs, chans), F32)
        p = jnp.ones((segs, chans), F32)
        for j in range(steps):
            a_j = across(a_s, j)
            h = a_j * h + across(b_s, j)
            p = p * a_j
            h_s[j] = h
            p_s[j] = p
        al = jnp.ones((1, chans), F32)
        be = jnp.zeros((1, chans), F32)
        als, bes = [al], [be]
        for s in range(segs):
            ps_, hs_ = p[s : s + 1, :], h[s : s + 1, :]
            be = ps_ * be + hs_
            al = ps_ * al
            als.append(al)
            bes.append(be)
        cown[layer, 0:1, :] = al
        cown[layer, 1:2, :] = be
        for k in range(1, BACK + 1):
            rcopy(cown.at[layer], cbuf.at[layer, k - 1], c_send.at[layer], c_recv.at[layer, k - 1], at_sp(k), tp)
        c_in = jnp.zeros((1, chans), F32)
        for k in range(BACK, 0, -1):
            wait(cbuf.at[layer, k - 1], c_recv.at[layer, k - 1])
            c_in = cbuf[layer, k - 1, 0:1, :] * c_in + cbuf[layer, k - 1, 1:2, :]
        carry = jnp.concatenate([als[s] * c_in + bes[s] for s in range(segs)], axis=0)
        for j in range(steps):
            value = h_s[j] + p_s[j] * carry
            for i in range(chans // 128):
                hid[i, pl.ds(j, segs, stride=steps), :] = value[:, i * 128 : (i + 1) * 128]
        return jnp.concatenate([hid[i].astype(BF16) for i in range(chans // 128)], axis=1)

    def layer_back(layer, hidden, state_chunk, big, arrived):
        m = 2 * layer + 1
        order = (2, 1, -1, 0)
        for j, d in enumerate(order):
            part = nt_dot(hidden, wrows(m, at_x(d, 1)))
            send_d[layer, j] = part.astype(BF16)
            rcopy(send_d.at[layer, j], recv_d.at[layer, j], ds.at[layer, j], dr.at[layer, j], sp, partner)

        def send_half(i, value, to):
            send_x[layer, i] = value.astype(BF16)
            rcopy(send_x.at[layer, i], recv_x.at[layer, i], xs.at[layer, i], xr.at[layer, i], sp, to)

        for j, d in enumerate(order):
            part = nt_dot(hidden, wrows(m, at_x(d)))
            wait(recv_d.at[layer, j], dr.at[layer, j])
            both = part + recv_d[layer, j].astype(F32)
            if j == 0:
                send_half(0, both[:hr], xp)
                send_half(1, both[hr:], xm)
            elif j == 1:
                send_half(2, both[hr:], xp)
                keep[:hr, :] = both[:hr]
            elif j == 2:
                send_half(3, both[:hr], xm)
                keep[hr:, :] = both[hr:]
            else:
                own[...] = both + state_chunk().astype(F32)
        for i, to in ((0, xp), (1, xm)):
            half = slice(0, hr) if i == 0 else slice(hr, rows)
            wait(recv_x.at[layer, i], xr.at[layer, i])
            send_half(4 + i, keep[half, :] + recv_x[layer, i].astype(F32), to)
        for i in (2, 3):
            wait(recv_x.at[layer, i], xr.at[layer, i])
        top = own[:hr, :] + recv_x[layer, 3].astype(F32)
        bottom = own[hr:, :] + recv_x[layer, 2].astype(F32)
        wait(recv_x.at[layer, 4], xr.at[layer, 4])
        big[tp, 0:hr, :] = (top + recv_x[layer, 4].astype(F32)).astype(BF16)
        wait(recv_x.at[layer, 5], xr.at[layer, 5])
        big[tp, hr:rows, :] = (bottom + recv_x[layer, 5].astype(F32)).astype(BF16)

        def to_partner(i, q):
            rcopy(big.at[q], big.at[q], ps.at[layer, i], pr.at[layer, i], sp, partner)

        for i, to in ((0, xp), (1, xm)):
            rcopy(big.at[tp], big.at[tp], gs.at[layer, i], gr.at[layer, i], sp, to)
        to_partner(0, tp)
        arrived(tp)
        for i, (q, to) in enumerate(((xm, xp), (xp, xm))):
            half = slice(0, hr) if i == 0 else slice(hr, rows)
            wait(big.at[q], gr.at[layer, i])
            rcopy(big.at[q, half, :], big.at[q, half, :], gs.at[layer, 2 + i], gr.at[layer, 2 + i], sp, to)
            to_partner(1 + i, q)
        wait(big.at[partner], pr.at[layer, 0])
        arrived(partner)
        for i, d in enumerate((-1, 1)):
            arrived(at_x(d))
            wait(big.at[at_x(d, 1)], pr.at[layer, 1 + i])
            arrived(at_x(d, 1))
        far = at_x(2)
        wait(big.at[far, 0:hr, :], gr.at[layer, 2])
        wait(big.at[far, hr:rows, :], gr.at[layer, 3])
        to_partner(3, far)
        arrived(far)
        wait(big.at[at_x(2, 1)], pr.at[layer, 3])
        arrived(at_x(2, 1))

    have(0)

    def project(q, _):
        acc[...] += jnp.dot(xg[q], wrows(0, q), preferred_element_type=F32)
        return 0

    lax.fori_loop(0, n_tp, project, 0)
    hidden = layer_front(0)
    have(1)
    have(2)
    have(3)
    ss[...] = jnp.zeros_like(ss)
    acc[...] = jnp.zeros_like(acc)

    def absorb(q):
        acc[...] += jnp.dot(scaled(1, x1[q], q), wrows(2, q), preferred_element_type=F32)

    def token_chunk():
        return tokens[:, pl.ds(pl.multiple_of(tp * cw, cw), cw)]

    layer_back(0, hidden, token_chunk, x1, absorb)

    hidden = layer_front(1)

    def write_out(q):
        pltpu.make_async_copy(
            outb.at[q], out.at[:, pl.ds(pl.multiple_of(q * cw, cw), cw)], o_sem.at[q]
        ).start()

    layer_back(1, hidden, lambda: x1[tp], outb, write_out)

    for q in range(n_tp):
        pltpu.make_async_copy(outb.at[q], out.at[:, q * cw : (q + 1) * cw], o_sem.at[q]).wait()
    for m in range(4):
        n_hops = n_z - 1
        wait(wbuf.at[m, :, 0 : n_hops * 5 * blk // 2], z_send.at[m])
        wait(wbuf.at[m, :, 0 : (3 + 3 * n_z) * blk // 2], y_send.at[m])
    wait(docs, d_sem.at[0])
    for layer in range(2):
        wait(cbuf.at[layer], c_send.at[layer])
        for j in range(4):
            wait(send_d.at[layer, j], ds.at[layer, j])
            wait(outb.at[j], ps.at[layer, j])
            wait(outb.at[j] if j < 2 else outb.at[j, 0:hr, :], gs.at[layer, j])
        for j in range(6):
            wait(send_x.at[layer, j], xs.at[layer, j])


def per_device(
    n_sp, tokens, documents, norm_gain, in_weight, conv_taps, conv_bias, recur_gate, input_gate,
    recur_bias, input_bias, decay_param, out_weight,
):
    rows, width = tokens.shape
    layers, blk, chans = in_weight.shape
    n_tp = 2 * NX
    cw = width // n_tp
    hr = rows // 2
    flat = (layers, chans, recur_gate.shape[3])
    vmem = pl.BlockSpec(memory_space=pltpu.VMEM)
    big = pltpu.VMEM((n_tp, rows, cw), BF16)
    square = pltpu.VMEM((rows, chans), F32)
    lanes = pltpu.VMEM((chans // 128, rows, 128), F32)
    strided = pltpu.VMEM((rows // 8, 8, chans), F32)
    dma = pltpu.SemaphoreType.DMA
    scratch = [
        pltpu.VMEM((4, 2, width, chans // 2), BF16),
        pltpu.VMEM((1, rows), jnp.int32),
        pltpu.VMEM((rows + 8, 128), F32),
        pltpu.VMEM((3, rows, 128), F32),
        pltpu.VMEM((layers, chans, 2 * chans), BF16),
        big,
        big,
        big,
        square,
        pltpu.VMEM((rows, 128), F32),
        pltpu.VMEM((rows + 8, chans), F32),
        pltpu.VMEM((layers, 8, chans), F32),
        lanes,
        lanes,
        strided,
        strided,
        lanes,
        pltpu.VMEM((layers, 2, chans), F32),
        pltpu.VMEM((layers, BACK, 2, chans), F32),
        pltpu.VMEM((layers, 4, rows, cw), BF16),
        pltpu.VMEM((layers, 4, rows, cw), BF16),
        pltpu.VMEM((layers, 6, hr, cw), BF16),
        pltpu.VMEM((layers, 6, hr, cw), BF16),
        pltpu.VMEM((rows, cw), F32),
        pltpu.VMEM((rows, cw), F32),
        dma((4, 2, n_sp // NY // 2 + 1, 2)),
        dma((4, 2)),
        dma((4,)),
        dma((4,)),
        dma((2,)),
        dma((layers, 2)),
        dma((layers, BACK)),
        dma((layers,)),
        dma((layers, 4)),
        dma((layers, 4)),
        dma((layers, 6)),
        dma((layers, 6)),
        dma((layers, 4)),
        dma((layers, 4)),
        dma((layers, 4)),
        dma((layers, 4)),
        dma((n_tp,)),
    ]
    return pl.pallas_call(
        functools.partial(kernel, n_sp),
        out_shape=jax.ShapeDtypeStruct((rows, width), BF16),
        in_specs=[vmem] * 12,
        out_specs=pl.BlockSpec(memory_space=pl.ANY),
        scratch_shapes=scratch,
        compiler_params=pltpu.CompilerParams(
            collective_id=0, has_side_effects=True, vmem_limit_bytes=56 * 1024 * 1024
        ),
    )(
        documents.reshape(1, rows), tokens, norm_gain, in_weight, conv_taps, conv_bias,
        recur_gate.reshape(flat), input_gate.reshape(flat), recur_bias, input_bias, decay_param, out_weight,
    )


def solution(mesh):
    return jax.shard_map(
        functools.partial(per_device, mesh.shape["sp"]),
        mesh=mesh,
        in_specs=(
            P("sp", None),
            P("sp"),
            P(),
            P(None, "sp", "tp"),
            P(None, None, "tp"),
            P(None, "tp"),
            P(None, "tp", None, None),
            P(None, "tp", None, None),
            P(None, "tp"),
            P(None, "tp"),
            P(None, "tp"),
            P(None, "tp", "sp"),
        ),
        out_specs=P("sp", None),
        check_vma=False,
    )
```

time: 460 us -> 186 us (0.40)
  waiting for transfers between devices: 303 us -> 0 us
  Pallas kernels: 0 us -> 181 us
  local copies, waits for them, and re-layouts: 43.1 us -> 4.73 us
  other arithmetic: 32.1 us -> 0 us
  blocking collectives: 31.6 us -> 0 us
  starting transfers between devices: 21.2 us -> 0 us
  between operations: 14.7 us -> 0.01 us
  matrix products: 11.5 us -> 0 us
    pallas_call x0 -> x1, Pallas kernels: none -> 181 us  [per_device(): pl.pallas_call(functools.partial(kernel, n_sp), out_shape=jax.ShapeDtypeS...]
    psum x2 -> x0, waiting for transfers between devices: 155 us -> none  [per_device(): lax.psum(partial_sum.astype(jnp.bfloat16), 'tp').astype(jnp.float32)]
    all_gather x1 -> x0, waiting for transfers between devices: 140 us -> none  [gather_turned(): lax.all_gather(both, axis, axis=0, tiled=True)]
    all_to_all x1 -> x0, blocking collectives: 31.6 us -> none  [from_everyone(): return lax.all_to_all(copies, axis, split_axis=0, concat_axis=0, tiled=True)]
    slice x155 -> x0, local copies, waits for them, and re-layouts: 29 us -> none  [the longest x104 15.8 us: per_device(): lax.associative_scan(combine, (decay_now, drive_term), axis=0)]
    concatenate x31 -> x0, other arithmetic: 12.3 us -> none  [the longest x27 11.6 us: per_device(): lax.associative_scan(combine, (decay_now, drive_term), axis=0)]
    all_to_all x1 -> x0, starting transfers between devices: 12.3 us -> none  [from_everyone(): return lax.all_to_all(copies, axis, split_axis=0, concat_axis=0, tiled=True)]
    dot_general x8 -> x0, matrix products: 11.5 us -> none  [the longest x2 7.27 us: per_device(): jnp.dot(hidden, whole_out[depth_at], preferred_element_type=jnp.float32)]
  transfers between devices with their start and end apart: 7 -> 0, of which waited for: 6 -> 0; matrix products, arithmetic and copies ran while one was open for 4% -> 0% of each run, Pallas kernels for 0% -> 0%
where the time goes in v1:
time: 186 us
  Pallas kernels  181 us (97%)
  local copies, waits for them, and re-layouts  4.73 us (3%)
    pallas_call x1, Pallas kernels, per_device(): pl.pallas_call(functools.partial(kernel, n_sp), out_shape=jax.ShapeDtypeS...  181 us
    unnamed x2, local copies, waits for them, and re-layouts  4.73 us

profile of v1, /device:TPU:1, one launch (start us, length us, event | category | flops | bytes accessed | tf_op | source)
XLA Modules:
  0.0 185.9 jit_solution(17406702145466702108)
XLA Ops:
  0.0 1.6 copy.13.w_out
  1.6 181.2 %shard_map.118 = bf16[256,4096]{1,0:T(8,128)(2,1)} custom-call(s32[1,256]{1,0:T(1,128)} %bitcast.5, bf16[256,4096]{1,0:T(8,128)(2,1)} %tokens.1, f32[2,4096]{1,0:T(2,128)} %gain.1, bf16[2,64,256]{2,1,0:T(8,128)(2,1)} %w_in.1, f32[2,4,256]{2,1,0:T(4,128)} %taps.1, f32[2,256]{1,0:T(2,128)} %conv_bias.1, bf16[2,256,64]{2,1,0:T(8,128)(2,1)} %bitcast.3, ...), custom_call_target="tpu_custom_call" | custom-call | tf_op jit(solution)/shard_map/pallas_call | solution.py:468
  182.8 3.1 %copy.15 = bf16[256,4096]{1,0:T(8,128)(2,1)} copy(bf16[256,4096]{1,0:T(8,128)(2,1)} %shard_map.118) | data formatting | bytes 4194304

commit v2 on v1

--- a/solution.py
+++ b/solution.py
@@ -15,7 +15,27 @@
 NY = 4
 NX = 4
 BACK = 8
-OFFSETS = (0, 4, 8, 12)
+SCHEDULE = {f"t{t}": [(0, t)] for t in range(9)}
+for t in range(3, 9):
+    SCHEDULE[f"t{t}"].append((1, t - 3))
+for t in range(6, 9):
+    SCHEDULE[f"t{t}"].append((2, t - 6))
+SCHEDULE |= {
+    "f0a": [(1, 6)],
+    "f0b": [(1, 7), (2, 3)],
+    "f0c": [(1, 8), (2, 4)],
+    "b0a": [(2, 5)],
+    "b0b": [(2, 6), (3, 0)],
+    "b0c": [(2, 7)],
+    "b0d": [(2, 8), (3, 1)],
+    "g0a": [(3, 2)],
+    "g0b": [(3, 3)],
+    "g0c": [(3, 4)],
+    "f1a": [(3, 5)],
+    "f1b": [(3, 6)],
+    "f1c": [(3, 7)],
+    "b1": [(3, 8)],
+}
 
 
 def nt_dot(a, b):
@@ -25,7 +45,7 @@
 def kernel(
     n_sp, docs, tokens, gain, w_in, taps, conv_bias, rgate, igate, rbias, ibias, decay, w_out, out,
     wbuf, pdoc, dext, masks, gm, xg, x1, outb, acc, ss, ext, tail, a_s, b_s, h_s, p_s, hid,
-    cown, cbuf, send_d, recv_d, send_x, recv_x, keep, own,
+    cown, cbuf, send_d, recv_d, send_x, recv_x, keep, own, part,
     z_recv, y_recv, z_send, y_send, d_sem, t_sem, c_recv, c_send, dr, ds, xr, xs, gr, gs, pr, ps, o_sem,
 ):
     rows, width = tokens.shape
@@ -74,13 +94,10 @@
     for to_sp, to_tp in partners:
         pl.semaphore_signal(barrier, inc=1, device_id=(to_sp, to_tp), device_id_type=MESH)
 
-    eye = (
-        lax.broadcasted_iota(jnp.int32, (blk, blk), 0) == lax.broadcasted_iota(jnp.int32, (blk, blk), 1)
-    ).astype(BF16)
     mine = pl.ds(pl.multiple_of(sp * blk, blk), blk)
     for layer in range(2):
         w = w_in[layer]
-        wt = nt_dot(eye, w_out[layer]).astype(BF16)
+        wt = w_out[layer]
         for h in range(2):
             lanes = slice(h * half_l, (h + 1) * half_l)
             wbuf[2 * layer, h, mine, :] = w[:, lanes]
@@ -151,18 +168,11 @@
             if s < last_step(m, d):
                 fwd_second(m, d, s + 1, zs[d])
 
-    done = [0]
-
-    def run_ticks(upto):
-        while done[0] < upto:
-            t = done[0]
-            for m in range(4):
-                if 0 <= t - OFFSETS[m] <= n_z // 2:
-                    tick(m, t - OFFSETS[m])
-            done[0] += 1
+    def run(point):
+        for m, step in SCHEDULE.get(point, ()):
+            tick(m, step)
 
     def have(m):
-        run_ticks(OFFSETS[m] + n_z // 2 + 1)
         wait(wbuf.at[m, 0, 0 : (n_z * 3) * blk], y_recv.at[m, 1])
 
     def wrows(m, q):
@@ -170,7 +180,7 @@
         return jnp.concatenate([wbuf[m, 0, r, :], wbuf[m, 1, r, :]], axis=1)
 
     rcopy(docs, pdoc, d_sem.at[0], d_sem.at[1], at_sp(1), tp)
-    run_ticks(1)
+    run("t0")
 
     ss[...] = jnp.zeros_like(ss)
     acc[...] = jnp.zeros_like(acc)
@@ -190,7 +200,7 @@
         return 0
 
     lax.fori_loop(0, n_tp, prepare, 0)
-    run_ticks(2)
+    run("t1")
 
     bd = rgate.shape[2]
     spread = (
@@ -205,7 +215,7 @@
         for i, g in enumerate((rgate, igate)):
             tiled = jnp.dot(g[layer], spread, preferred_element_type=F32)
             gm[layer, :, i * chans : (i + 1) * chans] = jnp.where(on_block, tiled, 0.0).astype(BF16)
-    run_ticks(3)
+    run("t2")
 
     wait(pdoc, d_sem.at[1])
     eye_r = (
@@ -234,6 +244,7 @@
         mixed = (acc[...] * r).astype(BF16).astype(F32)
         ext[8:, :] = mixed
         rcopy(ext.at[rows : rows + 8, :], tail.at[layer], t_sem.at[layer, 0], t_sem.at[layer, 1], at_sp(1), tp)
+        run(f"f{layer}a")
         wait(tail.at[layer], t_sem.at[layer, 1])
         wait(tail.at[layer], t_sem.at[layer, 0])
         ext[0:8, :] = tail[layer]
@@ -259,6 +270,7 @@
             series = 1.0 - (u * (1.0 / n)) * series
         gone = jnp.where(u < 0.35, u * series, 1.0 - jnp.exp(-u))
         put(b_s, jnp.sqrt(jnp.maximum(gone, 0.0)) * (ir * conv_f))
+        run(f"f{layer}b")
         h = jnp.zeros((segs, chans), F32)
         p = jnp.ones((segs, chans), F32)
         for j in range(steps):
@@ -280,6 +292,7 @@
         cown[layer, 1:2, :] = be
         for k in range(1, BACK + 1):
             rcopy(cown.at[layer], cbuf.at[layer, k - 1], c_send.at[layer], c_recv.at[layer, k - 1], at_sp(k), tp)
+        run(f"f{layer}c")
         c_in = jnp.zeros((1, chans), F32)
         for k in range(BACK, 0, -1):
             wait(cbuf.at[layer, k - 1], c_recv.at[layer, k - 1])
@@ -293,70 +306,104 @@
 
     def layer_back(layer, hidden, state_chunk, big, arrived):
         m = 2 * layer + 1
+        run(f"b{layer}")
+        have(m)
         order = (2, 1, -1, 0)
-        for j, d in enumerate(order):
-            part = nt_dot(hidden, wrows(m, at_x(d, 1)))
-            send_d[layer, j] = part.astype(BF16)
+
+        def for_partner(j):
+            send_d[layer, j] = nt_dot(hidden, wrows(m, at_x(order[j], 1))).astype(BF16)
             rcopy(send_d.at[layer, j], recv_d.at[layer, j], ds.at[layer, j], dr.at[layer, j], sp, partner)
+
+        def for_self(j):
+            part[j] = nt_dot(hidden, wrows(m, at_x(order[j])))
+
+        def of_chip(j):
+            wait(recv_d.at[layer, j], dr.at[layer, j])
+            return part[j] + recv_d[layer, j].astype(F32)
 
         def send_half(i, value, to):
             send_x[layer, i] = value.astype(BF16)
             rcopy(send_x.at[layer, i], recv_x.at[layer, i], xs.at[layer, i], xr.at[layer, i], sp, to)
 
-        for j, d in enumerate(order):
-            part = nt_dot(hidden, wrows(m, at_x(d)))
-            wait(recv_d.at[layer, j], dr.at[layer, j])
-            both = part + recv_d[layer, j].astype(F32)
-            if j == 0:
-                send_half(0, both[:hr], xp)
-                send_half(1, both[hr:], xm)
-            elif j == 1:
-                send_half(2, both[hr:], xp)
-                keep[:hr, :] = both[:hr]
-            elif j == 2:
-                send_half(3, both[:hr], xm)
-                keep[hr:, :] = both[hr:]
-            else:
-                own[...] = both + state_chunk().astype(F32)
+        for_partner(0)
+        for_self(0)
+        for_partner(1)
+        both = of_chip(0)
+        send_half(0, both[:hr], xp)
+        send_half(1, both[hr:], xm)
+        for_self(1)
+        for_partner(2)
+        run(f"b{layer}a")
+        both = of_chip(1)
+        send_half(2, both[hr:], xp)
+        keep[:hr, :] = both[:hr]
+        for_self(2)
+        for_partner(3)
+        both = of_chip(2)
+        send_half(3, both[:hr], xm)
+        keep[hr:, :] = both[hr:]
+        for_self(3)
+        run(f"b{layer}b")
+        own[...] = of_chip(3) + state_chunk().astype(F32)
+        run(f"b{layer}c")
         for i, to in ((0, xp), (1, xm)):
             half = slice(0, hr) if i == 0 else slice(hr, rows)
             wait(recv_x.at[layer, i], xr.at[layer, i])
             send_half(4 + i, keep[half, :] + recv_x[layer, i].astype(F32), to)
+        run(f"b{layer}d")
         for i in (2, 3):
             wait(recv_x.at[layer, i], xr.at[layer, i])
         top = own[:hr, :] + recv_x[layer, 3].astype(F32)
         bottom = own[hr:, :] + recv_x[layer, 2].astype(F32)
+
+        def half_of(q, h):
+            return big.at[q, h * hr : (h + 1) * hr, :]
+
+        def to_x(i, q, h, to):
+            rcopy(half_of(q, h), half_of(q, h), gs.at[layer, i], gr.at[layer, i], sp, to)
+
+        def to_partner(i, q):
+            rcopy(big.at[q], big.at[q], ps.at[layer, i], pr.at[layer, i], sp, partner)
+
         wait(recv_x.at[layer, 4], xr.at[layer, 4])
         big[tp, 0:hr, :] = (top + recv_x[layer, 4].astype(F32)).astype(BF16)
+        to_x(0, tp, 0, xp)
         wait(recv_x.at[layer, 5], xr.at[layer, 5])
         big[tp, hr:rows, :] = (bottom + recv_x[layer, 5].astype(F32)).astype(BF16)
-
-        def to_partner(i, q):
-            rcopy(big.at[q], big.at[q], ps.at[layer, i], pr.at[layer, i], sp, partner)
-
-        for i, to in ((0, xp), (1, xm)):
-            rcopy(big.at[tp], big.at[tp], gs.at[layer, i], gr.at[layer, i], sp, to)
+        to_x(1, tp, 1, xm)
+        to_x(2, tp, 1, xp)
+        to_x(3, tp, 0, xm)
         to_partner(0, tp)
+        if layer == 0:
+            have(2)
         arrived(tp)
-        for i, (q, to) in enumerate(((xm, xp), (xp, xm))):
-            half = slice(0, hr) if i == 0 else slice(hr, rows)
-            wait(big.at[q], gr.at[layer, i])
-            rcopy(big.at[q, half, :], big.at[q, half, :], gs.at[layer, 2 + i], gr.at[layer, 2 + i], sp, to)
-            to_partner(1 + i, q)
+        run(f"g{layer}a")
+        wait(half_of(xm, 0), gr.at[layer, 0])
+        to_x(4, xm, 0, xp)
+        wait(half_of(xp, 1), gr.at[layer, 1])
+        to_x(5, xp, 1, xm)
+        wait(half_of(xm, 1), gr.at[layer, 2])
+        to_partner(1, xm)
+        wait(half_of(xp, 0), gr.at[layer, 3])
+        to_partner(2, xp)
+        run(f"g{layer}b")
         wait(big.at[partner], pr.at[layer, 0])
         arrived(partner)
         for i, d in enumerate((-1, 1)):
             arrived(at_x(d))
             wait(big.at[at_x(d, 1)], pr.at[layer, 1 + i])
             arrived(at_x(d, 1))
+        run(f"g{layer}c")
         far = at_x(2)
-        wait(big.at[far, 0:hr, :], gr.at[layer, 2])
-        wait(big.at[far, hr:rows, :], gr.at[layer, 3])
+        wait(half_of(far, 0), gr.at[layer, 4])
+        wait(half_of(far, 1), gr.at[layer, 5])
         to_partner(3, far)
         arrived(far)
         wait(big.at[at_x(2, 1)], pr.at[layer, 3])
         arrived(at_x(2, 1))
 
+    for t in range(3, 9):
+        run(f"t{t}")
     have(0)
 
     def project(q, _):
@@ -365,9 +412,6 @@
 
     lax.fori_loop(0, n_tp, project, 0)
     hidden = layer_front(0)
-    have(1)
-    have(2)
-    have(3)
     ss[...] = jnp.zeros_like(ss)
     acc[...] = jnp.zeros_like(acc)
 
@@ -400,8 +444,8 @@
         for j in range(4):
             wait(send_d.at[layer, j], ds.at[layer, j])
             wait(outb.at[j], ps.at[layer, j])
-            wait(outb.at[j] if j < 2 else outb.at[j, 0:hr, :], gs.at[layer, j])
         for j in range(6):
+            wait(outb.at[j, 0:hr, :], gs.at[layer, j])
             wait(send_x.at[layer, j], xs.at[layer, j])
 
 
@@ -447,6 +491,7 @@
         pltpu.VMEM((layers, 6, hr, cw), BF16),
         pltpu.VMEM((rows, cw), F32),
         pltpu.VMEM((rows, cw), F32),
+        pltpu.VMEM((4, rows, cw), F32),
         dma((4, 2, n_sp // NY // 2 + 1, 2)),
         dma((4, 2)),
         dma((4,)),
@@ -459,8 +504,8 @@
         dma((layers, 4)),
         dma((layers, 6)),
         dma((layers, 6)),
-        dma((layers, 4)),
-        dma((layers, 4)),
+        dma((layers, 6)),
+        dma((layers, 6)),
         dma((layers, 4)),
         dma((layers, 4)),
         dma((n_tp,)),
@@ -476,7 +521,7 @@
         ),
     )(
         documents.reshape(1, rows), tokens, norm_gain, in_weight, conv_taps, conv_bias,
-        recur_gate.reshape(flat), input_gate.reshape(flat), recur_bias, input_bias, decay_param, out_weight,
+        recur_gate.reshape(flat), input_gate.reshape(flat), recur_bias, input_bias, decay_param, jnp.swapaxes(out_weight, 1, 2),
     )
 
 

time: 186 us -> 149 us (0.80)
  Pallas kernels: 181 us -> 146 us
    pallas_call x1, Pallas kernels: 181 us -> 146 us  [per_device(): pl.pallas_call(functools.partial(kernel, n_sp), out_shape=jax.ShapeDtypeS...]
    unnamed x2 -> x1, local copies, waits for them, and re-layouts: 4.73 us -> 3.13 us
where the time goes in v2:
time: 149 us
  Pallas kernels  146 us (98%)
  local copies, waits for them, and re-layouts  3.13 us (2%)
    pallas_call x1, Pallas kernels, per_device(): pl.pallas_call(functools.partial(kernel, n_sp), out_shape=jax.ShapeDtypeS...  146 us
    unnamed x1, local copies, waits for them, and re-layouts  3.13 us

profile of v2, /device:TPU:1, one launch (start us, length us, event | category | flops | bytes accessed | tf_op | source)
XLA Modules:
  0.0 148.9 jit_solution(3420001292249362110)
XLA Ops:
  0.0 145.8 %shard_map.118 = bf16[256,4096]{1,0:T(8,128)(2,1)} custom-call(s32[1,256]{1,0:T(1,128)} %bitcast.7, bf16[256,4096]{1,0:T(8,128)(2,1)} %tokens.1, f32[2,4096]{1,0:T(2,128)} %gain.1, bf16[2,64,256]{2,1,0:T(8,128)(2,1)} %w_in.1, f32[2,4,256]{2,1,0:T(4,128)} %taps.1, f32[2,256]{1,0:T(2,128)} %conv_bias.1, bf16[2,256,64]{2,1,0:T(8,128)(2,1)} %bitcast.4, ...), custom_call_target="tpu_custom_call" | custom-call | tf_op jit(solution)/shard_map/pallas_call | solution.py:513
  145.8 3.1 %copy.14 = bf16[256,4096]{1,0:T(8,128)(2,1)} copy(bf16[256,4096]{1,0:T(8,128)(2,1)} %shard_map.118) | data formatting | bytes 4194304

commit v3 on v2

--- a/solution.py
+++ b/solution.py
@@ -15,27 +15,25 @@
 NY = 4
 NX = 4
 BACK = 8
-SCHEDULE = {f"t{t}": [(0, t)] for t in range(9)}
-for t in range(3, 9):
-    SCHEDULE[f"t{t}"].append((1, t - 3))
-for t in range(6, 9):
-    SCHEDULE[f"t{t}"].append((2, t - 6))
-SCHEDULE |= {
-    "f0a": [(1, 6)],
-    "f0b": [(1, 7), (2, 3)],
-    "f0c": [(1, 8), (2, 4)],
-    "b0a": [(2, 5)],
-    "b0b": [(2, 6), (3, 0)],
-    "b0c": [(2, 7)],
-    "b0d": [(2, 8), (3, 1)],
-    "g0a": [(3, 2)],
-    "g0b": [(3, 3)],
-    "g0c": [(3, 4)],
-    "f1a": [(3, 5)],
-    "f1b": [(3, 6)],
-    "f1c": [(3, 7)],
-    "b1": [(3, 8)],
+SCHEDULE = {
+    "w0": [(0, 0)],
+    "w1": [(0, 1), (1, 0)],
+    "w2": [(0, 2), (1, 1)],
+    "w3": [(0, 3), (1, 2)],
+    "w4": [(0, 4), (1, 3)],
+    "w5": [(0, 5), (1, 4), (2, 0)],
+    "w6": [(0, 6), (1, 5), (2, 1)],
+    "w7": [(0, 7), (1, 6), (2, 2), (3, 0)],
+    "w8": [(0, 8), (1, 7), (2, 3), (3, 1)],
+    "hp": [(1, 8), (2, 4), (3, 2)],
+    "f0c": [(2, 5), (3, 3)],
+    "f0d": [(2, 6), (3, 4)],
+    "b0c": [(2, 7), (3, 5)],
+    "b0d": [(2, 8), (3, 6)],
+    "g0a": [(3, 7)],
+    "g0h": [(3, 8)],
 }
+TAIL = 16
 
 
 def nt_dot(a, b):
@@ -46,7 +44,7 @@
     n_sp, docs, tokens, gain, w_in, taps, conv_bias, rgate, igate, rbias, ibias, decay, w_out, out,
     wbuf, pdoc, dext, masks, gm, xg, x1, outb, acc, ss, ext, tail, a_s, b_s, h_s, p_s, hid,
     cown, cbuf, send_d, recv_d, send_x, recv_x, keep, own, part,
-    z_recv, y_recv, z_send, y_send, d_sem, t_sem, c_recv, c_send, dr, ds, xr, xs, gr, gs, pr, ps, o_sem,
+    z0_recv, z_recv, y_recv, z_send, y_send, d_sem, t_sem, c_recv, c_send, dr, ds, xr, xs, gr, gs, pr, ps, o_sem,
 ):
     rows, width = tokens.shape
     chans = taps.shape[2]
@@ -90,7 +88,8 @@
     barrier = pltpu.get_barrier_semaphore()
     partners = [(at_y(1), tp), (at_y(-1), tp), (at_y(2), tp), (at_z(1), tp), (at_z(-1), tp)]
     partners += [(sp, xp), (sp, xm), (sp, partner)]
-    partners += [(at_sp(d), tp) for k in range(1, BACK + 1) for d in (k, -k)]
+    partners += [(at_sp(d), tp) for k in range(2, BACK + 1) for d in (k, -k)]
+    partners += [(at_sp(d), lax.rem(tp + k, n_tp)) for k in range(n_tp) for d in (1, -1)]
     for to_sp, to_tp in partners:
         pl.semaphore_signal(barrier, inc=1, device_id=(to_sp, to_tp), device_id_type=MESH)
 
@@ -121,52 +120,44 @@
                 piece = wbuf.at[m, h, mine, :]
                 rcopy(piece, piece, y_send.at[m], y_recv.at[m, h], at_y(d), tp)
 
-    def pass_first(m, d, zz):
-        to = at_z(1 if d == 0 else -1)
-        s_sem = z_send.at[m]
-        return to, s_sem
-
-    def fwd_first(m, d, s, zz):
-        to, s_sem = pass_first(m, d, zz)
-        r = block_rows(zz, y)
-        piece = wbuf.at[m, :, r, :] if m == 0 else wbuf.at[m, 1, r, :]
-        rcopy(piece, piece, s_sem, z_recv.at[m, d, s, 0], to, tp)
-
-    def fwd_second(m, d, s, zz):
-        to, s_sem = pass_first(m, d, zz)
+    def pieces(m, zz):
+        own_col = block_rows(zz, y)
         if m == 0:
-            for dy in (1, -1, 2):
-                piece = wbuf.at[m, 0, block_rows(zz, lax.rem(y + dy + NY, NY)), :]
-                rcopy(piece, piece, s_sem, z_recv.at[m, d, s, 1], to, tp)
-        else:
-            piece = wbuf.at[m, 0, z_rows(zz), :]
-            rcopy(piece, piece, s_sem, z_recv.at[m, d, s, 1], to, tp)
-
-    first_rows = [2 * blk, blk, blk, blk]
-    second_rows = [3 * blk, 4 * blk, 4 * blk, 4 * blk]
+            parts = [wbuf.at[m, 1, own_col, :], wbuf.at[m, 0, own_col, :]]
+            parts += [wbuf.at[m, 0, block_rows(zz, lax.rem(y + dy + NY, NY)), :] for dy in (1, -1, 2)]
+            return parts
+        return [wbuf.at[m, 1, own_col, :], wbuf.at[m, 0, z_rows(zz), :]]
+
+    def pass_on(m, d, s, zz, i):
+        piece = pieces(m, zz)[i]
+        sem = z0_recv.at[d, s, i] if m == 0 else z_recv.at[m - 1, d, s, i]
+        rcopy(piece, piece, z_send.at[m], sem, at_z(1 if d == 0 else -1), tp)
 
     def tick(m, s):
+        count = 5 if m == 0 else 2
         if s == 0:
-            for d in range(2):
-                fwd_first(m, d, 1, z)
+            early = 2 if m == 0 else 1
+            for i in range(early):
+                for d in range(2):
+                    pass_on(m, d, 1, z, i)
             start_y(m)
             wait(wbuf.at[m, 0, 0 : 3 * blk], y_recv.at[m, 0])
-            for d in range(2):
-                fwd_second(m, d, 1, z)
+            for i in range(early, count):
+                for d in range(2):
+                    pass_on(m, d, 1, z, i)
             return
         live = [d for d in range(2) if s <= last_step(m, d)]
         zs = {0: lax.rem(z - s + n_z, n_z), 1: lax.rem(z + s, n_z)}
-        for d in live:
-            wait(wbuf.at[m, 0, 0 : first_rows[m]], z_recv.at[m, d, s, 0])
-            if s < last_step(m, d):
-                fwd_first(m, d, s + 1, zs[d])
-            piece = wbuf.at[m, 1, block_rows(zs[d], y), :]
-            for dy in (1, -1, 2):
-                rcopy(piece, piece, y_send.at[m], y_recv.at[m, 1], at_y(dy), tp)
-        for d in live:
-            wait(wbuf.at[m, 0, 0 : second_rows[m]], z_recv.at[m, d, s, 1])
-            if s < last_step(m, d):
-                fwd_second(m, d, s + 1, zs[d])
+        for i in range(count):
+            for d in live:
+                sem = z0_recv.at[d, s, i] if m == 0 else z_recv.at[m - 1, d, s, i]
+                wait(wbuf.at[m, 0, 0 : (4 * blk if m > 0 and i == 1 else blk)], sem)
+                if s < last_step(m, d):
+                    pass_on(m, d, s + 1, zs[d], i)
+                if i == 0:
+                    piece = pieces(m, zs[d])[0]
+                    for dy in (1, -1, 2):
+                        rcopy(piece, piece, y_send.at[m], y_recv.at[m, 1], at_y(dy), tp)
 
     def run(point):
         for m, step in SCHEDULE.get(point, ()):
@@ -180,27 +171,30 @@
         return jnp.concatenate([wbuf[m, 0, r, :], wbuf[m, 1, r, :]], axis=1)
 
     rcopy(docs, pdoc, d_sem.at[0], d_sem.at[1], at_sp(1), tp)
-    run("t0")
+    rcopy(tokens.at[rows - TAIL :, :], tail.at[0], t_sem.at[0, 0], t_sem.at[0, 1], at_sp(1), tp)
+    run("w0")
 
     ss[...] = jnp.zeros_like(ss)
     acc[...] = jnp.zeros_like(acc)
 
     def scaled(layer, values, q):
-        v = values.astype(F32)
+        columns = pl.ds(pl.multiple_of(q * cw, cw), cw)
+        v = jnp.concatenate([tail[layer, :, columns].astype(F32), values.astype(F32)], axis=0)
         sq = v * v
         part = sq[:, 0:128]
         for i in range(1, cw // 128):
             part = part + sq[:, i * 128 : (i + 1) * 128]
         ss[...] += part
-        g = gain[layer : layer + 1, pl.ds(pl.multiple_of(q * cw, cw), cw)]
+        g = gain[layer : layer + 1, columns]
         return (v * g).astype(BF16)
 
     def prepare(q, _):
         xg[q] = scaled(0, tokens[:, pl.ds(pl.multiple_of(q * cw, cw), cw)], q)
         return 0
 
+    wait(tail.at[0], t_sem.at[0, 1])
     lax.fori_loop(0, n_tp, prepare, 0)
-    run("t1")
+    run("w1")
 
     bd = rgate.shape[2]
     spread = (
@@ -215,7 +209,7 @@
         for i, g in enumerate((rgate, igate)):
             tiled = jnp.dot(g[layer], spread, preferred_element_type=F32)
             gm[layer, :, i * chans : (i + 1) * chans] = jnp.where(on_block, tiled, 0.0).astype(BF16)
-    run("t2")
+    run("w2")
 
     wait(pdoc, d_sem.at[1])
     eye_r = (
@@ -241,20 +235,15 @@
 
     def layer_front(layer):
         r = lax.rsqrt(jnp.sum(ss[...], axis=1, keepdims=True) * (1.0 / width) + EPS)
-        mixed = (acc[...] * r).astype(BF16).astype(F32)
-        ext[8:, :] = mixed
-        rcopy(ext.at[rows : rows + 8, :], tail.at[layer], t_sem.at[layer, 0], t_sem.at[layer, 1], at_sp(1), tp)
+        ext[...] = (acc[...] * r).astype(BF16).astype(F32)
         run(f"f{layer}a")
-        wait(tail.at[layer], t_sem.at[layer, 1])
-        wait(tail.at[layer], t_sem.at[layer, 0])
-        ext[0:8, :] = tail[layer]
 
         def wide(mask):
             return jnp.concatenate([mask] * (chans // 128), axis=1)
 
-        conv = conv_bias[layer : layer + 1, :] + taps[layer, 0:1, :] * mixed
+        conv = conv_bias[layer : layer + 1, :] + taps[layer, 0:1, :] * ext[TAIL:, :]
         for k in range(1, 4):
-            conv = conv + wide(masks[k - 1]) * (taps[layer, k : k + 1, :] * ext[8 - k : 8 - k + rows, :])
+            conv = conv + wide(masks[k - 1]) * (taps[layer, k : k + 1, :] * ext[TAIL - k : TAIL - k + rows, :])
         conv_b = conv.astype(BF16)
         conv_f = conv_b.astype(F32)
         logits = jnp.dot(conv_b, gm[layer], preferred_element_type=F32)
@@ -270,7 +259,6 @@
             series = 1.0 - (u * (1.0 / n)) * series
         gone = jnp.where(u < 0.35, u * series, 1.0 - jnp.exp(-u))
         put(b_s, jnp.sqrt(jnp.maximum(gone, 0.0)) * (ir * conv_f))
-        run(f"f{layer}b")
         h = jnp.zeros((segs, chans), F32)
         p = jnp.ones((segs, chans), F32)
         for j in range(steps):
@@ -297,6 +285,7 @@
         for k in range(BACK, 0, -1):
             wait(cbuf.at[layer, k - 1], c_recv.at[layer, k - 1])
             c_in = cbuf[layer, k - 1, 0:1, :] * c_in + cbuf[layer, k - 1, 1:2, :]
+        run(f"f{layer}d")
         carry = jnp.concatenate([als[s] * c_in + bes[s] for s in range(segs)], axis=0)
         for j in range(steps):
             value = h_s[j] + p_s[j] * carry
@@ -306,7 +295,6 @@
 
     def layer_back(layer, hidden, state_chunk, big, arrived):
         m = 2 * layer + 1
-        run(f"b{layer}")
         have(m)
         order = (2, 1, -1, 0)
 
@@ -333,7 +321,7 @@
         send_half(1, both[hr:], xm)
         for_self(1)
         for_partner(2)
-        run(f"b{layer}a")
+        run(f"b{layer}b")
         both = of_chip(1)
         send_half(2, both[hr:], xp)
         keep[:hr, :] = both[:hr]
@@ -343,7 +331,6 @@
         send_half(3, both[:hr], xm)
         keep[hr:, :] = both[hr:]
         for_self(3)
-        run(f"b{layer}b")
         own[...] = of_chip(3) + state_chunk().astype(F32)
         run(f"b{layer}c")
         for i, to in ((0, xp), (1, xm)):
@@ -375,25 +362,35 @@
         to_x(3, tp, 0, xm)
         to_partner(0, tp)
         if layer == 0:
-            have(2)
-        arrived(tp)
+            for k in range(n_tp):
+                rcopy(
+                    big.at[tp, rows - TAIL : rows, :],
+                    tail.at[1, :, pl.ds(pl.multiple_of(tp * cw, cw), cw)],
+                    t_sem.at[1, 0], t_sem.at[1, 1], at_sp(1), lax.rem(tp + k, n_tp),
+                )
+        held = [tp]
         run(f"g{layer}a")
         wait(half_of(xm, 0), gr.at[layer, 0])
         to_x(4, xm, 0, xp)
         wait(half_of(xp, 1), gr.at[layer, 1])
         to_x(5, xp, 1, xm)
+        run(f"g{layer}h")
         wait(half_of(xm, 1), gr.at[layer, 2])
         to_partner(1, xm)
         wait(half_of(xp, 0), gr.at[layer, 3])
         to_partner(2, xp)
         run(f"g{layer}b")
         wait(big.at[partner], pr.at[layer, 0])
-        arrived(partner)
+        held += [partner, xm, xp]
         for i, d in enumerate((-1, 1)):
-            arrived(at_x(d))
             wait(big.at[at_x(d, 1)], pr.at[layer, 1 + i])
-            arrived(at_x(d, 1))
+            held.append(at_x(d, 1))
         run(f"g{layer}c")
+        if layer == 0:
+            have(2)
+            wait(tail.at[1], t_sem.at[1, 1])
+        for q in held:
+            arrived(q)
         far = at_x(2)
         wait(half_of(far, 0), gr.at[layer, 4])
         wait(half_of(far, 1), gr.at[layer, 5])
@@ -403,8 +400,9 @@
         arrived(at_x(2, 1))
 
     for t in range(3, 9):
-        run(f"t{t}")
+        run(f"w{t}")
     have(0)
+    run("hp")
 
     def project(q, _):
         acc[...] += jnp.dot(xg[q], wrows(0, q), preferred_element_type=F32)
@@ -440,6 +438,7 @@
         wait(wbuf.at[m, :, 0 : (3 + 3 * n_z) * blk // 2], y_send.at[m])
     wait(docs, d_sem.at[0])
     for layer in range(2):
+        wait(tail.at[layer], t_sem.at[layer, 0])
         wait(cbuf.at[layer], c_send.at[layer])
         for j in range(4):
             wait(send_d.at[layer, j], ds.at[layer, j])
@@ -461,7 +460,6 @@
     flat = (layers, chans, recur_gate.shape[3])
     vmem = pl.BlockSpec(memory_space=pltpu.VMEM)
     big = pltpu.VMEM((n_tp, rows, cw), BF16)
-    square = pltpu.VMEM((rows, chans), F32)
     lanes = pltpu.VMEM((chans // 128, rows, 128), F32)
     strided = pltpu.VMEM((rows // 8, 8, chans), F32)
     dma = pltpu.SemaphoreType.DMA
@@ -471,13 +469,13 @@
         pltpu.VMEM((rows + 8, 128), F32),
         pltpu.VMEM((3, rows, 128), F32),
         pltpu.VMEM((layers, chans, 2 * chans), BF16),
+        pltpu.VMEM((n_tp, rows + TAIL, cw), BF16),
         big,
         big,
-        big,
-        square,
-        pltpu.VMEM((rows, 128), F32),
-        pltpu.VMEM((rows + 8, chans), F32),
-        pltpu.VMEM((layers, 8, chans), F32),
+        pltpu.VMEM((rows + TAIL, chans), F32),
+        pltpu.VMEM((rows + TAIL, 128), F32),
+        pltpu.VMEM((rows + TAIL, chans), F32),
+        pltpu.VMEM((layers, TAIL, width), BF16),
         lanes,
         lanes,
         strided,
@@ -492,7 +490,8 @@
         pltpu.VMEM((rows, cw), F32),
         pltpu.VMEM((rows, cw), F32),
         pltpu.VMEM((4, rows, cw), F32),
-        dma((4, 2, n_sp // NY // 2 + 1, 2)),
+        dma((2, n_sp // NY // 2 + 1, 5)),
+        dma((3, 2, n_sp // NY // 2 + 1, 2)),
         dma((4, 2)),
         dma((4,)),
         dma((4,)),

time: 149 us -> 144 us (0.966)
  Pallas kernels: 146 us -> 140 us
    pallas_call x1, Pallas kernels: 146 us -> 140 us  [per_device(): pl.pallas_call(functools.partial(kernel, n_sp), out_shape=jax.ShapeDtypeS...]
where the time goes in v3:
time: 144 us; the launch traced here: 143 us
  Pallas kernels  140 us (97%)
  local copies, waits for them, and re-layouts  3.13 us (2%)
    pallas_call x1, Pallas kernels, per_device(): pl.pallas_call(functools.partial(kernel, n_sp), out_shape=jax.ShapeDtypeS...  140 us
    unnamed x1, local copies, waits for them, and re-layouts  3.13 us

profile of v3, /device:TPU:1, one launch (start us, length us, event | category | flops | bytes accessed | tf_op | source)
XLA Modules:
  0.0 143.4 jit_solution(8800649560634957705)
XLA Ops:
  0.0 140.3 %shard_map.118 = bf16[256,4096]{1,0:T(8,128)(2,1)} custom-call(s32[1,256]{1,0:T(1,128)} %bitcast.7, bf16[256,4096]{1,0:T(8,128)(2,1)} %tokens.1, f32[2,4096]{1,0:T(2,128)} %gain.1, bf16[2,64,256]{2,1,0:T(8,128)(2,1)} %w_in.1, f32[2,4,256]{2,1,0:T(4,128)} %taps.1, f32[2,256]{1,0:T(2,128)} %conv_bias.1, bf16[2,256,64]{2,1,0:T(8,128)(2,1)} %bitcast.4, ...), custom_call_target="tpu_custom_call" | custom-call | tf_op jit(solution)/shard_map/pallas_call | solution.py:512
  140.3 3.1 %copy.14 = bf16[256,4096]{1,0:T(8,128)(2,1)} copy(bf16[256,4096]{1,0:T(8,128)(2,1)} %shard_map.118) | data formatting | bytes 4194304

commit v4 on v3

--- a/solution.py
+++ b/solution.py
@@ -425,13 +425,13 @@
 
     def write_out(q):
         pltpu.make_async_copy(
-            outb.at[q], out.at[:, pl.ds(pl.multiple_of(q * cw, cw), cw)], o_sem.at[q]
+            outb.at[q], out.at[q], o_sem.at[q]
         ).start()
 
     layer_back(1, hidden, lambda: x1[tp], outb, write_out)
 
     for q in range(n_tp):
-        pltpu.make_async_copy(outb.at[q], out.at[:, q * cw : (q + 1) * cw], o_sem.at[q]).wait()
+        pltpu.make_async_copy(outb.at[q], out.at[q], o_sem.at[q]).wait()
     for m in range(4):
         n_hops = n_z - 1
         wait(wbuf.at[m, :, 0 : n_hops * 5 * blk // 2], z_send.at[m])
@@ -509,9 +509,9 @@
         dma((layers, 4)),
         dma((n_tp,)),
     ]
-    return pl.pallas_call(
+    chunks = pl.pallas_call(
         functools.partial(kernel, n_sp),
-        out_shape=jax.ShapeDtypeStruct((rows, width), BF16),
+        out_shape=jax.ShapeDtypeStruct((n_tp, rows, cw), BF16),
         in_specs=[vmem] * 12,
         out_specs=pl.BlockSpec(memory_space=pl.ANY),
         scratch_shapes=scratch,
@@ -522,6 +522,34 @@
         documents.reshape(1, rows), tokens, norm_gain, in_weight, conv_taps, conv_bias,
         recur_gate.reshape(flat), input_gate.reshape(flat), recur_bias, input_bias, decay_param, jnp.swapaxes(out_weight, 1, 2),
     )
+    return laid_out(chunks)
+
+
+def copy_kernel(src, dst, buf, i_sem, o_sem):
+    n, rows, cw = buf.shape
+    for q in range(n):
+        pltpu.make_async_copy(src.at[q], buf.at[q], i_sem.at[q]).start()
+    for q in range(n):
+        pltpu.make_async_copy(src.at[q], buf.at[q], i_sem.at[q]).wait()
+        pltpu.make_async_copy(buf.at[q], dst.at[:, q * cw : (q + 1) * cw], o_sem.at[q]).start()
+    for q in range(n):
+        pltpu.make_async_copy(buf.at[q], dst.at[:, q * cw : (q + 1) * cw], o_sem.at[q]).wait()
+
+
+def laid_out(chunks):
+    n, rows, cw = chunks.shape
+    anywhere = pl.BlockSpec(memory_space=pl.ANY)
+    return pl.pallas_call(
+        copy_kernel,
+        out_shape=jax.ShapeDtypeStruct((rows, n * cw), BF16),
+        in_specs=[anywhere],
+        out_specs=anywhere,
+        scratch_shapes=[
+            pltpu.VMEM((n, rows, cw), BF16),
+            pltpu.SemaphoreType.DMA((n,)),
+            pltpu.SemaphoreType.DMA((n,)),
+        ],
+    )(chunks)
 
 
 def solution(mesh):

time: 144 us -> 143 us (level)
  local copies, waits for them, and re-layouts: 3.13 us -> 0 us
  Pallas kernels: 140 us -> 143 us
    unnamed x1 -> x0, local copies, waits for them, and re-layouts: 3.13 us -> none
    pallas_call x0 -> x1, Pallas kernels: none -> 2.4 us  [laid_out(): pl.pallas_call(copy_kernel, out_shape=jax.ShapeDtypeStruct((rows, n * cw)...]
where the time goes in v4:
time: 143 us
  Pallas kernels  143 us (100%)
    pallas_call x1, Pallas kernels, per_device(): pl.pallas_call(functools.partial(kernel, n_sp), out_shape=jax.ShapeDtypeS...  140 us

profile of v4, /device:TPU:1, one launch (start us, length us, event | category | flops | bytes accessed | tf_op | source)
XLA Modules:
  0.0 142.6 jit_solution(17905072366275280584)
XLA Ops:
  0.0 140.2 %shard_map.118.src = bf16[8,256,512]{2,1,0:T(8,128)(2,1)} custom-call(s32[1,256]{1,0:T(1,128)} %bitcast.7, bf16[256,4096]{1,0:T(8,128)(2,1)} %tokens.1, f32[2,4096]{1,0:T(2,128)} %gain.1, bf16[2,64,256]{2,1,0:T(8,128)(2,1)} %w_in.1, f32[2,4,256]{2,1,0:T(4,128)} %taps.1, f32[2,256]{1,0:T(2,128)} %conv_bias.1, bf16[2,256,64]{2,1,0:T(8,128)(2,1)} %bitcast.4, ...), custom_call_target="tpu_custom_call" | custom-call | tf_op jit(solution)/shard_map/pallas_call | solution.py:512
  140.2 2.4 %shard_map.119 = bf16[256,4096]{1,0:T(8,128)(2,1)} custom-call(bf16[8,256,512]{2,1,0:T(8,128)(2,1)} %shard_map.118.src), custom_call_target="tpu_custom_call" | custom-call | tf_op jit(solution)/shard_map/pallas_call | solution.py:542
